TPU v7x, 32 devices: a whole 2x2x4 slice. The times are simulated.
32 devices in a mesh: grp: 2 (over x), ep: 16 (over z, y, core).
Axes of the slice: x: 2, y: 2, z: 4, core: 2. Of those that a mesh axis runs over, the one named last changes fastest.
Arguments:
- tokens: bfloat16 [32, 2048], P(('grp', 'ep')), parts along dimension 0, may hold values from -6 to 6
- cache_latent: bfloat16 [32, 3072, 512], P(('grp', 'ep')), parts along dimension 0, may hold values from -6 to 6
- cache_rope: bfloat16 [32, 32, 3072], P(('grp', 'ep')), parts along dimension 0, may hold values from -1000 to 1000
- lengths: int32 [32], P(('grp', 'ep')), parts along dimension 0, may hold values from 384 to 3072, as said below
- w_query: bfloat16 [2048, 1536], P('ep'), may hold values from -0.125 to 0.125
- w_latent: bfloat16 [2048, 512], P('ep'), may hold values from -0.125 to 0.125
- w_rope: bfloat16 [2048, 32], P('ep'), may hold values from -0.125 to 0.125
- w_absorb: bfloat16 [512, 1024], replicated, may hold values from -0.25 to 0.25
- w_value: bfloat16 [512, 1024], replicated, may hold values from -0.25 to 0.25
- w_output: bfloat16 [1024, 2048], P('ep'), may hold values from -0.1875 to 0.1875
- gain_attn: float32 [2048], replicated, may hold values from 0.1 to 1.9
- gain_latent: float32 [512], replicated, may hold values from 0.1 to 1.9
- gain_moe: float32 [2048], replicated, may hold values from 0.1 to 1.9
- routes: int32 [32, 2], P(('grp', 'ep')), parts along dimension 0, may hold values from 0 to 15, all different within a row; in each aligned block of 16 rows (0 to 15, 16 to 31, ...) at most 4 rows name the same one
- route_scores: float32 [32, 2], P(('grp', 'ep')), parts along dimension 0, may hold values from 0.2 to 1
- w_gate: bfloat16 [16, 2048, 512], P('ep'), may hold values from -0.125 to 0.125
- w_up: bfloat16 [16, 2048, 512], P('ep'), may hold values from -0.125 to 0.125
- w_down: bfloat16 [16, 512, 2048], P('ep'), may hold values from -0.25 to 0.25
Outputs:
- mixed: bfloat16 [32, 2048], P(('grp', 'ep')), parts along dimension 0
- new_latent: bfloat16 [32, 512], P(('grp', 'ep')), parts along dimension 0
- new_rope: bfloat16 [32, 32], P(('grp', 'ep')), parts along dimension 0
There are 2 independent parts, one for each index of `grp`. A program takes and returns all parts, laid end to end along the dimension named above; an argument that names none is the same for every part. Nothing has to cross between parts.
Inputs may be any that keep to these rules, and one draw needn't show every extreme that they name: `routes`: each row names 2 different experts; over one part's 16 tokens no expert is named by more than 4 rows, a bound that some block reaches. `lengths`: some sequence has all 3072 positions filled.
All inputs are finite; a program needn't handle non-finite values.
Results may differ from a plain program's by a relative error of at most 0.013.
Values may be sent and summed in bfloat16 or wider, within the bound.
A program may use at most 64 MiB of HBM per device.

v0:
```python
import functools
import jax
import jax.numpy as jnp
from jax import lax
from jax.experimental import pallas as pl
from jax.experimental.pallas import tpu as pltpu
from jax.sharding import PartitionSpec as P

HEADS = 16
NOPE = 64
ROPE = 32
VDIM = 64
EPS = 1e-06
THETA = 10000.0
LANES = 128
F32 = jnp.float32
BF16 = jnp.bfloat16
MESH = pl.DeviceIdType.MESH


def dot(a, b):
    return jnp.dot(a, b, preferred_element_type=F32)


def dot_t(a, b):
    return lax.dot_general(a, b, (((1,), (1,)), ((), ())), preferred_element_type=F32)


def rms_scale(values, gain):
    return values * lax.rsqrt(jnp.mean(values * values, axis=-1, keepdims=True) + EPS) * gain


def iota(shape, dim):
    return lax.broadcasted_iota(jnp.int32, shape, dim)


def ones_where(mask):
    return jnp.where(mask, 1.0, 0.0).astype(BF16)


def kernel(
    n,
    tok_ref, table_ref, g_attn_ref, g_lat_ref, g_moe_ref, len_ref, route_ref, score_ref,
    cache_hbm, crope_hbm, wq_hbm, wl_hbm, wr_hbm, wa_hbm, wv_hbm, wo_hbm, wg_hbm, wu_hbm, wd_hbm,
    mixed_ref, nlat_ref, nrope_ref,
    cache, crope, wq, wl, wr, wa, wv, wo, wg, wu, wd,
    send1, recv1, rows1, send2, recv2, send3, recv3, rows3, send4, recv4, send5, recv5, rows5,
    send6, recv6, local_sem, link_sem,
):
    me = lax.axis_index("ep")
    pairs = [
        (wq_hbm, wq), (wl_hbm, wl), (wr_hbm, wr), (wa_hbm, wa), (crope_hbm.at[0], crope),
        (cache_hbm.at[0], cache), (wv_hbm, wv), (wo_hbm, wo),
        (wg_hbm.at[0], wg), (wu_hbm.at[0], wu), (wd_hbm.at[0], wd),
    ]
    loads = [pltpu.make_async_copy(a, b, local_sem.at[i]) for i, (a, b) in enumerate(pairs)]
    for load in loads:
        load.start()
    (l_wq, l_wl, l_wr, l_wa, l_crope, l_cache, l_wv, l_wo, l_wg, l_wu, l_wd) = loads

    barrier = pltpu.get_barrier_semaphore()

    def greet(k, carry):
        pl.semaphore_signal(
            barrier, inc=1, device_id={"ep": lax.rem(me + k, n)}, device_id_type=MESH
        )
        return carry

    lax.fori_loop(1, n, greet, 0)

    def copy(phase, source, target, peer, slot):
        return pltpu.make_async_remote_copy(
            src_ref=source(peer),
            dst_ref=target.at[slot],
            send_sem=link_sem.at[phase, 0, peer],
            recv_sem=link_sem.at[phase, 1, slot],
            device_id={"ep": peer},
            device_id_type=MESH,
        )

    def send(phase, source, target):
        def step(k, carry):
            copy(phase, source, target, lax.rem(me + k, n), me).start()
            return carry

        lax.fori_loop(1, n, step, 0)

    def receive(phase, source, target):
        def step(k, carry):
            peer = lax.rem(me + n - k, n)
            copy(phase, source, target, peer, peer).wait_recv()
            return carry

        lax.fori_loop(1, n, step, 0)

    def sent(phase, source, target):
        def step(k, carry):
            peer = lax.rem(me + k, n)
            copy(phase, source, target, peer, peer).wait_send()
            return carry

        lax.fori_loop(1, n, step, 0)

    def gather_rows(buffer, rows):
        for t in range(n):
            rows[t : t + 1, :] = buffer[t]

    tokens = tok_ref[...].astype(F32)
    normed = rms_scale(tokens, g_attn_ref[...]).astype(BF16).astype(F32)
    depth = wq.shape[0]
    for t in range(n):
        send1[t] = normed[:, t * depth : (t + 1) * depth]
    recv1[me] = send1[me]
    pl.semaphore_wait(barrier, n - 1)
    src1 = lambda peer: send1.at[peer]
    send(0, src1, recv1)
    qw, lw, rw = wq.shape[1], wl.shape[1], wr.shape[1]
    l_wq.wait()
    l_wl.wait()
    l_wr.wait()
    receive(0, src1, recv1)
    gather_rows(recv1, rows1)
    rows = rows1[...].astype(BF16)
    part_q = dot(rows, wq[...])
    part_l = dot(rows, wl[...])
    part_r = dot(rows, wr[...])
    for t in range(n):
        send2[t, :, :qw] = part_q[t : t + 1]
        send2[t, :, qw : qw + lw] = part_l[t : t + 1]
        send2[t, :, qw + lw : qw + lw + rw] = part_r[t : t + 1]
    recv2[me] = send2[me]
    src2 = lambda peer: send2.at[peer]
    send(1, src2, recv2)
    sel = jnp.concatenate([ones_where(iota((NOPE + ROPE, LANES), 0) == iota((NOPE + ROPE, LANES), 1))] * HEADS, axis=0)
    head_width = NOPE + ROPE
    own_q = iota((HEADS, qw), 1) - head_width * iota((HEADS, qw), 0)
    own_q = (own_q >= 0) & (own_q < head_width)
    spread = ones_where((iota((LANES, HEADS * NOPE), 1) & (NOPE - 1)) == iota((LANES, HEADS * NOPE), 0))
    own_n = iota((HEADS, HEADS * NOPE), 1) - NOPE * iota((HEADS, HEADS * NOPE), 0)
    own_n = (own_n >= 0) & (own_n < NOPE)
    half = ROPE // 2
    lane = iota((LANES, ROPE), 1)
    swapped = jnp.where(lane < half, lane + half, lane - half)
    pick = ones_where(iota((LANES, ROPE), 0) == NOPE + lane)
    pick_swap = ones_where(iota((LANES, ROPE), 0) == NOPE + swapped)
    swap = ones_where(iota((ROPE, ROPE), 0) == swapped[:ROPE])
    cosine, sine = table_ref[0:1, :], table_ref[1:2, :]
    receive(1, src2, recv2)
    summed = jnp.sum(recv2[:, :, : qw + lw + LANES], axis=0)
    latent_raw = summed[:, qw : qw + lw].astype(BF16).astype(F32)
    new_latent = rms_scale(latent_raw, g_lat_ref[...]).astype(BF16)
    nlat_ref[...] = new_latent
    new_latent = new_latent.astype(F32)
    rope_raw = jnp.broadcast_to(summed[:, qw + lw : qw + lw + rw].astype(BF16).astype(F32), (HEADS, rw))
    new_rope = rope_raw * cosine + dot(rope_raw.astype(BF16), swap) * sine
    new_rope = new_rope.astype(BF16)
    nrope_ref[...] = new_rope[0:1, :]
    new_rope = new_rope.astype(F32)
    query = jnp.broadcast_to(summed[:, :qw].astype(BF16).astype(F32), (HEADS, qw))
    query = jnp.where(own_q, query, 0.0).astype(BF16)
    heads = dot(query, sel).astype(BF16)
    q_pe = (dot(heads, pick) * cosine + dot(heads, pick_swap) * sine).astype(BF16)
    q_diag = jnp.where(own_n, dot(heads, spread), 0.0).astype(BF16)
    l_wa.wait()
    q_abs = dot_t(q_diag, wa[...]).astype(BF16)
    scale = (NOPE + ROPE) ** (-0.5)
    l_crope.wait()
    l_cache.wait()
    past = (dot_t(q_abs, cache[...]) + dot(q_pe, crope[...])) * scale
    fresh = (
        jnp.sum(q_abs.astype(F32) * new_latent, axis=-1, keepdims=True)
        + jnp.sum(q_pe.astype(F32) * new_rope, axis=-1, keepdims=True)
    ) * scale
    past = jnp.where(iota(past.shape, 1) < len_ref[0], past, -jnp.inf)
    top = jnp.maximum(jnp.max(past, axis=-1, keepdims=True), fresh)
    e_past = jnp.exp(past - top)
    e_new = jnp.exp(fresh - top)
    total = jnp.sum(e_past, axis=-1, keepdims=True) + e_new
    inverse = 1.0 / total
    p_past = (e_past * inverse).astype(BF16)
    p_new = (e_new * inverse).astype(BF16).astype(F32)
    attended = (dot(p_past, cache[...]) + p_new * new_latent).astype(BF16)
    l_wv.wait()
    values = dot(attended, wv[...])
    values = jnp.sum(jnp.where(own_n, values, 0.0), axis=0, keepdims=True).astype(BF16).astype(F32)
    for t in range(send3.shape[0]):
        send3[t] = values[:, t * LANES : (t + 1) * LANES]
    width = wo.shape[0]
    group = LANES // width
    recv3[me] = send3[me // group]
    src3 = lambda peer: send3.at[peer // group]
    send(2, src3, recv3)
    l_wo.wait()
    cut = ones_where(iota((LANES, width), 0) == iota((LANES, width), 1) + width * lax.rem(me, group))
    receive(2, src3, recv3)
    gather_rows(recv3, rows3)
    rows = dot(rows3[...].astype(BF16), cut).astype(BF16)
    part = dot(rows, wo[...])
    for t in range(n):
        send4[t] = part[t : t + 1]
    recv4[me] = send4[me]
    src4 = lambda peer: send4.at[peer]
    send(3, src4, recv4)
    receive(3, src4, recv4)
    resid = (tokens + jnp.sum(recv4[...], axis=0)).astype(BF16).astype(F32)
    moe_in = rms_scale(resid, g_moe_ref[...]).astype(BF16).astype(F32)
    send5[0] = moe_in
    recv5[me] = moe_in
    src5 = lambda peer: send5.at[0]
    send(4, src5, recv5)
    l_wg.wait()
    l_wu.wait()
    l_wd.wait()
    receive(4, src5, recv5)
    gather_rows(recv5, rows5)
    rows = rows5[...].astype(BF16)
    gate = dot(rows, wg[...])
    upper = dot(rows, wu[...])
    hidden = (jax.nn.silu(gate) * upper).astype(BF16)
    result = dot(hidden, wd[...]).astype(BF16).astype(F32)
    for t in range(n):
        send6[t] = result[t : t + 1]
    recv6[me] = send6[me]
    src6 = lambda peer: send6.at[peer]
    send(5, src6, recv6)
    topk = route_ref.shape[1]
    weight = score_ref[0, 0]
    for k in range(1, topk):
        weight = weight + score_ref[0, k]
    receive(5, src6, recv6)
    moe_sum = jnp.zeros_like(resid)
    for k in range(topk):
        moe_sum = moe_sum + (jnp.full(resid.shape, score_ref[0, k]) / weight) * recv6[route_ref[0, k]]
    mixed_ref[...] = (resid + moe_sum).astype(BF16)
    sent(0, src1, recv1)
    sent(1, src2, recv2)
    sent(2, src3, recv3)
    sent(3, src4, recv4)
    sent(4, src5, recv5)
    sent(5, src6, recv6)


def body(
    tokens, cache_latent, cache_rope, lengths, w_query, w_latent, w_rope, w_absorb, w_value,
    w_output, gain_attn, gain_latent, gain_moe, routes, route_scores, w_gate, w_up, w_down,
):
    n = lax.axis_size("ep")
    d = tokens.shape[1]
    total = w_query.shape[1] + w_latent.shape[1] + LANES
    inverse = THETA ** (-jnp.arange(0, ROPE, 2).astype(F32) / ROPE)
    angle = lengths.astype(F32)[:, None] * inverse[None, :]
    cosine, sine = jnp.cos(angle), jnp.sin(angle)
    table = jnp.concatenate(
        [jnp.concatenate([cosine, cosine], axis=1), jnp.concatenate([-sine, sine], axis=1)], axis=0
    )
    vmem = pl.BlockSpec(memory_space=pltpu.VMEM)
    smem = pl.BlockSpec(memory_space=pltpu.SMEM)
    hbm = pl.BlockSpec(memory_space=pl.ANY)

    def like(a):
        return pltpu.VMEM(a.shape[-2:], a.dtype)

    big = [w_query, w_latent, w_rope, w_absorb, w_value, w_output, w_gate, w_up, w_down]
    depth = w_query.shape[0]
    tiles = w_value.shape[1] // LANES
    row = lambda count, wide: pltpu.VMEM((count, 1, wide), F32)
    return pl.pallas_call(
        functools.partial(kernel, n),
        out_shape=(
            jax.ShapeDtypeStruct(tokens.shape, BF16),
            jax.ShapeDtypeStruct((1, w_latent.shape[1]), BF16),
            jax.ShapeDtypeStruct((1, w_rope.shape[1]), BF16),
        ),
        in_specs=[vmem] * 5 + [smem] * 3 + [hbm] * 11,
        out_specs=(vmem, vmem, vmem),
        scratch_shapes=[like(cache_latent), like(cache_rope)]
        + [like(a) for a in big]
        + [
            row(n, depth), row(n, depth), pltpu.VMEM((n, depth), F32),
            row(n, total), row(n, total),
            row(tiles, LANES), row(n, LANES), pltpu.VMEM((n, LANES), F32),
            row(n, d), row(n, d),
            row(1, d), row(n, d), pltpu.VMEM((n, d), F32),
            row(n, d), row(n, d),
            pltpu.SemaphoreType.DMA((11,)),
            pltpu.SemaphoreType.DMA((6, 2, n)),
        ],
        compiler_params=pltpu.CompilerParams(
            collective_id=0, has_side_effects=True, vmem_limit_bytes=56 * 1024 * 1024
        ),
    )(
        tokens, table, gain_attn[None, :], gain_latent[None, :], gain_moe[None, :], lengths, routes,
        route_scores, cache_latent, cache_rope, w_query, w_latent, w_rope, w_absorb, w_value,
        w_output, w_gate, w_up, w_down,
    )


def solution(mesh):
    rows = P(("grp", "ep"), None)
    cube = P(("grp", "ep"), None, None)
    split = P("ep", None)
    placed = (
        rows, cube, cube, P(("grp", "ep")), split, split, split, P(), P(), split, P(), P(), P(),
        rows, rows, P("ep", None, None), P("ep", None, None), P("ep", None, None),
    )
    return jax.shard_map(
        body, mesh=mesh, in_specs=placed, out_specs=(rows, rows, rows), check_vma=False
    )
```

profile of v0, /device:TPU:0, one launch (start us, length us, event | category | flops | bytes accessed | tf_op | source)
XLA Modules:
  0.0 48.6 jit_solution(12127241191113294940)
XLA Ops:
  1.3 0.1 fusion
  1.4 0.6 %maximum_maximum_fusion.table_ref = f32[2,32]{1,0:T(2,128)} fusion(f32[1,16]{1,0:T(1,128)S(1)} %get-tuple-element.3, f32[1,16]{1,0:T(1,128)S(1)} %fusion.2, f32[1,16]{1,0:T(1,128)S(1)} %get-tuple-element.4), kind=kLoop, calls=%fused_computation | loop fusion | flops 192 | bytes 448 | tf_op jit(solution)/shard_map/concatenate | solution.py:253
  2.0 1.4 %copy.21.wr_hbm = bf16[128,32]{1,0:T(8,128)(2,1)} copy(bf16[128,32]{0,1:T(8,128)(2,1)} %param.24) | data formatting | bytes 16384 | tf_op args[6]
  3.4 41.5 %shard_map.193 = (bf16[1,2048]{1,0:T(2,128)(2,1)}, bf16[1,512]{1,0:T(2,128)(2,1)}, bf16[1,32]{1,0:T(2,128)(2,1)}) custom-call(bf16[1,2048]{1,0:T(2,128)(2,1)} %tok_ref.1, f32[2,32]{1,0:T(2,128)} %maximum_maximum_fusion.table_ref, f32[1,2048]{1,0:T(1,128)} %bitcast.4, f32[1,512]{1,0:T(1,128)} %bitcast.6, f32[1,2048]{1,0:T(1,128)} %bitcast.5, ...), custom_call_target="tpu_custom_call" | custom-call | tf_op jit(solution)/shard_map/pallas_call | solution.py:267
  45.0 1.3 %copy.26 = bf16[1,2048]{1,0:T(2,128)(2,1)} copy(bf16[1,2048]{1,0:T(2,128)(2,1)} %get-tuple-element.8) | data formatting | bytes 8192
  46.3 1.2 %copy.27 = bf16[1,512]{1,0:T(2,128)(2,1)} copy(bf16[1,512]{1,0:T(2,128)(2,1)} %get-tuple-element.9) | data formatting | bytes 2048
  47.5 1.1 %copy.28 = bf16[1,32]{1,0:T(2,128)(2,1)} copy(bf16[1,32]{1,0:T(2,128)(2,1)} %get-tuple-element.10) | data formatting | bytes 128
  (1 shorter events, 0.0 us)
where the time goes:
time: 49 us; the launch traced here: 48.6 us
  Pallas kernels  41.5 us (85%)
  local copies, waits for them, and re-layouts  5.06 us (10%)
  between operations  1.3 us (3%)
  other arithmetic  0.75 us (2%)
    pallas_call x1, Pallas kernels, body(): pl.pallas_call(functools.partial(kernel, n), out_shape=(jax.ShapeDtypeStr...  41.5 us
    unnamed x4, local copies, waits for them, and re-layouts  5.06 us

commit v1 on v0

v1 whole, which is shorter than its diff:
```python
import functools
import math
import jax
import jax.numpy as jnp
from jax import lax
from jax.experimental import pallas as pl
from jax.experimental.pallas import tpu as pltpu
from jax.sharding import PartitionSpec as P

HEADS = 16
NOPE = 64
ROPE = 32
VDIM = 64
EPS = 1e-06
THETA = 10000.0
LANES = 128
CHUNKS = 2
EXACT = 8
FIRST = 3
F32 = jnp.float32
BF16 = jnp.bfloat16
MESH = pl.DeviceIdType.MESH


def dot(a, b):
    return jnp.dot(a, b, preferred_element_type=F32)


def dot_t(a, b):
    return lax.dot_general(a, b, (((1,), (1,)), ((), ())), preferred_element_type=F32)


def iota(shape, dim):
    return lax.broadcasted_iota(jnp.int32, shape, dim)


def ones_where(mask):
    return jnp.where(mask, 1.0, 0.0).astype(BF16)


def rms_dense(values, gain, size):
    total = jnp.sum(jnp.sum(values * values, axis=1, keepdims=True), axis=0, keepdims=True)
    return values * lax.rsqrt(total * (1.0 / size) + EPS) * gain


def rope_tables(position):
    half = ROPE // 2
    lane = iota((1, LANES), 1) & (ROPE - 1)
    step = lane & (half - 1)
    inverse = jnp.zeros((1, LANES), F32)
    for i in range(half):
        inverse = jnp.where(step == i, THETA ** (-2.0 * i / ROPE), inverse)
    angle = position.astype(F32) * inverse
    sine = jnp.sin(angle)
    return jnp.cos(angle), jnp.where(lane < half, -sine, sine)


def rotate(values, cosine, sine):
    half = ROPE // 2
    low = (iota(values.shape, 1) & (ROPE - 1)) < half
    swapped = jnp.where(low, pltpu.roll(values, LANES - half, 1), pltpu.roll(values, half, 1))
    return values * cosine + swapped * sine


def split_heads(heads):
    group = heads * (NOPE + ROPE)
    src, col = iota((group, group), 0), iota((group, group), 1)
    first = (NOPE + ROPE) * (col // NOPE) + (col & (NOPE - 1))
    rest = col - heads * NOPE
    second = (NOPE + ROPE) * (rest // ROPE) + NOPE + (rest & (ROPE - 1))
    return ones_where(src == jnp.where(col < heads * NOPE, first, second))


def rows_to_lanes(values, first, count, heads):
    return [jnp.broadcast_to(values[first + r : first + r + 1, :], (heads, LANES)) for r in range(count)]


def kernel(
    n, hubs,
    tok_hbm, g_attn_hbm, g_lat_hbm, g_moe_hbm, len_hbm, route_hbm, score_hbm,
    cache_hbm, crope_hbm, wq_hbm, wl_hbm, wr_hbm, wa_hbm, wv_hbm, wo_hbm, wg_hbm, wu_hbm, wd_hbm,
    mixed_ref, nlat_ref, nrope_ref,
    tok, g_attn, g_lat, g_moe, length, route, score,
    cache, wq, wl, wr, wa, wv, wo, wg, wu, wd, wqn, wocol, cache_t, wa_t, dense,
    send1, recv1, stage, send2, recv2, send2r, recv2r, stage3, send3, recv3, send4, recv4,
    send6, recv6, local_sem, link_sem, hub_sem,
):
    me = lax.axis_index("ep")
    barrier = pltpu.get_barrier_semaphore()
    upper = me // (n // 2)

    def far_first(k):
        return upper * k + (1 - upper) * (n - 1 - k)

    def each_peer(act):
        own = far_first(me)

        def step(k, carry):
            act(far_first(k))
            return carry

        lax.fori_loop(0, own, step, 0)
        lax.fori_loop(own + 1, n, step, 0)

    each_peer(
        lambda peer: pl.semaphore_signal(barrier, inc=1, device_id={"ep": peer}, device_id_type=MESH)
    )
    depth, width = wq_hbm.shape[0], wo_hbm.shape[0]
    share = LANES // depth
    cut = width * FIRST // 32 * 8
    mine = pl.ds(pl.multiple_of(depth * lax.rem(me, share), depth), depth)
    block = me // share
    tall = tok.shape[1] // LANES
    cols = tok.shape[1] // hubs
    per_hub = cols // LANES
    base = (n - 2 * hubs) // 2

    def hub_device(h):
        return base + 2 * h + 1

    def near_first(i):
        return upper * (hubs - 1 - i) + (1 - upper) * i

    my_hub = (me - base) // 2
    is_hub = (lax.rem(me, 2) == 1) & (me >= base) & (me < base + 2 * hubs)

    def columns(h):
        return pl.ds(pl.multiple_of(h * cols, cols), cols)

    def band(owner, size):
        return pl.ds(pl.multiple_of(owner * size, size), size)

    if share > 1:
        for w in (wq, wl, wr):
            w[...] = jnp.zeros_like(w)
    pairs = [
        (tok_hbm, tok), (g_attn_hbm, g_attn), (len_hbm, length), (wq_hbm, wq.at[mine]),
        (wl_hbm, wl.at[mine]), (wr_hbm, wr if share == 1 else wr.at[mine]), (wo_hbm, wo),
        (g_lat_hbm, g_lat), (g_moe_hbm, g_moe), (route_hbm, route), (score_hbm, score),
        (cache_hbm.at[0], cache), (wa_hbm, wa), (crope_hbm.at[0], cache_t.at[wl_hbm.shape[1] :]), (wv_hbm, wv),
        (wg_hbm.at[0], wg), (wu_hbm.at[0], wu), (wd_hbm.at[0], wd),
    ]
    loads = [pltpu.make_async_copy(a, b, local_sem.at[i]) for i, (a, b) in enumerate(pairs)]
    for load in loads:
        load.start()
    (
        l_tok, l_ga, l_len, l_wq, l_wl, l_wr, l_wo, l_gl, l_gm, l_route, l_score, l_cache, l_wa,
        l_crope, l_wv, l_wg, l_wu, l_wd,
    ) = loads

    def launch(peer, source, target, sent, received):
        pltpu.make_async_remote_copy(
            src_ref=source,
            dst_ref=target,
            send_sem=sent,
            recv_sem=received,
            device_id={"ep": peer},
            device_id_type=MESH,
        ).start()

    def send(phase, source, target):
        each_peer(
            lambda peer: launch(
                peer, source(peer), target, link_sem.at[0, phase], link_sem.at[1, phase]
            )
        )

    def await_bytes(ref, sem):
        pltpu.make_async_copy(ref, ref, sem).wait()

    def drain(side, phase, target):
        await_bytes(target.at[pl.ds(0, (n - 1) * (target.shape[0] // n))], link_sem.at[side, phase])

    def each_hub(act):
        for i in range(hubs):
            h = near_first(hubs - 1 - i)

            @pl.when(me != hub_device(h))
            def _():
                act(h)

    def reshard(half):
        low, high = (cut, width) if half else (0, cut)
        rows = pl.ds(pl.multiple_of(me * width + low, 8), high - low)
        source = lambda h: wo.at[low:high, columns(h)]
        each_hub(
            lambda h: launch(
                hub_device(h), source(h), wocol.at[rows], link_sem.at[0, 4 + half],
                link_sem.at[1, 4 + half],
            )
        )

        @pl.when(is_hub)
        def _():
            wocol[rows, :] = wo[low:high, columns(my_hub)]

    l_tok.wait()
    l_ga.wait()
    tokens = tok[...].astype(F32)
    for r in range(tall):
        dense[r : r + 1, :] = tokens[:, r * LANES : (r + 1) * LANES]
    tokens = dense[...]
    normed = rms_dense(tokens, g_attn[...], tok.shape[1]).astype(BF16).astype(F32)
    for r in range(tall):
        send1[r] = normed[r : r + 1, :]
    pl.semaphore_wait(barrier, n - 1)
    send(0, lambda peer: send1.at[peer // share], recv1.at[me])
    recv1[me] = send1[block]
    l_wo.wait()
    reshard(0)

    qw, lw = wq.shape[1], wl.shape[1]
    tiles = wv.shape[1] // LANES
    slot = send3.shape[1]
    for h in range(hubs):
        stage3[h * slot + tiles : h * slot + tiles + per_hub, :] = tokens[
            h * per_hub : (h + 1) * per_hub, :
        ]
    l_wq.wait()
    few = LANES // ROPE
    order = split_heads(few)
    span = few * (NOPE + ROPE)
    nope_rows, pe_rows, lat_rows = HEADS * NOPE // LANES, HEADS * ROPE // LANES, lw // LANES
    for g in range(HEADS // few):
        moved = dot(wq[:, g * span : (g + 1) * span], order).astype(BF16)
        wqn[:, g * few * NOPE : (g + 1) * few * NOPE] = moved[:, : few * NOPE]
        start = HEADS * NOPE + g * LANES
        wqn[:, start : start + LANES] = moved[:, few * NOPE :]
    l_len.wait()
    cosine, sine = rope_tables(jnp.full((1, LANES), length[0]))
    l_wl.wait()
    l_wr.wait()
    edge = 2 * LANES
    same = ones_where(iota((edge, edge), 0) == iota((edge, edge), 1))

    def turn(source, target):
        for i in range(source.shape[0] // edge):
            for j in range(source.shape[1] // edge):
                part = source[i * edge : (i + 1) * edge, j * edge : (j + 1) * edge]
                target[j * edge : (j + 1) * edge, i * edge : (i + 1) * edge] = dot_t(same, part).astype(BF16)

    l_cache.wait()
    turn(cache, cache_t)
    drain(1, 0, recv1)
    rows = jnp.concatenate([recv1[t] for t in range(n)], axis=0).astype(BF16)
    wide = (qw + lw) // LANES
    part_q = dot(rows, wqn[...])
    for j in range(qw // LANES):
        stage[pl.ds(j, n, stride=wide), :] = part_q[:, j * LANES : (j + 1) * LANES]
    part_l = dot(rows, wl[...])
    for j in range(lat_rows):
        stage[pl.ds(qw // LANES + j, n, stride=wide), :] = part_l[:, j * LANES : (j + 1) * LANES]
    part_r = dot_t(rows, wr[...]) if share == 1 else dot(rows, wr[...])
    for j in range(pe_rows):
        at = (nope_rows + j) * LANES
        send2r[pl.ds(j, n, stride=EXACT), :] = part_q[:, at : at + LANES]
    part_r = jnp.concatenate([part_r, jnp.zeros((n, LANES - ROPE), F32)], axis=1)
    send2r[pl.ds(pe_rows, n, stride=EXACT), :] = part_r
    send2[...] = stage[...].astype(BF16).reshape(send2.shape)

    def send_sums(peer):
        launch(
            peer, send2r.at[band(peer, EXACT)], recv2r.at[band(me, EXACT)], link_sem.at[0, 2],
            link_sem.at[1, 2],
        )
        launch(peer, send2.at[peer], recv2.at[me], link_sem.at[0, 1], link_sem.at[1, 1])

    each_peer(send_sums)
    recv2[me] = send2[me]
    recv2r[band(me, EXACT), :] = send2r[band(me, EXACT), :]
    drain(0, 0, recv1)
    l_gl.wait()
    l_wa.wait()
    turn(wa, wa_t)
    l_crope.wait()
    l_wv.wait()
    head = iota((HEADS, LANES), 0)
    lane = iota((HEADS, LANES), 1)
    drain(1, 1, recv2)
    drain(1, 2, recv2r)
    reshard(1)
    summed = recv2[0].astype(F32)
    exact = recv2r[:EXACT, :]
    for t in range(1, n):
        summed = summed + recv2[t].astype(F32)
        exact = exact + recv2r[t * EXACT : (t + 1) * EXACT, :]
    exact = exact.astype(BF16).astype(F32)
    summed = summed.astype(BF16).astype(F32)
    first = nope_rows + pe_rows
    new_latent = rms_dense(summed[first:, :], g_lat[...], lw).astype(BF16).astype(F32)
    rotated = rotate(exact, cosine, sine)
    new_rope = rotated[pe_rows : pe_rows + 1, :].astype(BF16)
    for r in range(lat_rows):
        nlat_ref[:, r * LANES : (r + 1) * LANES] = new_latent[r : r + 1, :].astype(BF16)
    nrope_ref[...] = new_rope[:, :ROPE]
    new_rope = new_rope.astype(F32)
    per = LANES // NOPE
    q_diag = jnp.concatenate(
        [
            jnp.where(head == per * r + lane // NOPE, row, 0.0)
            for r, row in enumerate(rows_to_lanes(summed, 0, nope_rows, HEADS))
        ],
        axis=1,
    ).astype(BF16)
    q_abs = dot(q_diag, wa_t[...]).astype(BF16)
    q_pe = jnp.zeros((HEADS, LANES), F32)
    for r, row in enumerate(rows_to_lanes(rotated, 0, pe_rows, HEADS)):
        q_pe = jnp.where(head == few * r + lane // ROPE, row, q_pe)
    shift = LANES // 2
    while shift >= ROPE:
        q_pe = q_pe + pltpu.roll(q_pe, shift, 1)
        shift //= 2
    q_pe = q_pe[:, :ROPE].astype(BF16)
    unit = (NOPE + ROPE) ** (-0.5) * math.log2(math.e)
    lat_row = jnp.concatenate(rows_to_lanes(new_latent, 0, lat_rows, HEADS), axis=1)
    fresh = jnp.sum(q_abs.astype(F32) * lat_row, axis=-1, keepdims=True) + jnp.sum(
        q_pe.astype(F32) * new_rope[:, :ROPE], axis=-1, keepdims=True
    )
    chunk = cache.shape[0] // CHUNKS
    query = jnp.concatenate([q_abs, q_pe], axis=1)
    pasts = [dot(query, cache_t[:, c * chunk : (c + 1) * chunk]) for c in range(CHUNKS)]
    tops, sums, outs = [], [], []
    for c, past in enumerate(pasts):
        past = jnp.where(iota(past.shape, 1) < length[0] - c * chunk, past, -jnp.inf)
        top = jnp.maximum(jnp.max(past, axis=-1, keepdims=True), fresh)
        e_past = jnp.exp2((past - top) * unit)
        tops.append(top)
        sums.append(jnp.sum(e_past, axis=-1, keepdims=True))
        outs.append(dot(e_past.astype(BF16), cache[c * chunk : (c + 1) * chunk, :]))
    top = functools.reduce(jnp.maximum, tops)
    e_new = jnp.exp2((fresh - top) * unit)
    total, mixed = e_new, e_new * lat_row
    for peak, part, out in zip(tops, sums, outs):
        weight = jnp.exp2((peak - top) * unit)
        total = total + part * weight
        mixed = mixed + out * weight
    attended = (mixed / total).astype(BF16)
    values = dot(attended, wv[...])
    for j in range(tiles):
        part = values[:, j * LANES : (j + 1) * LANES]
        part = jnp.where(head == (LANES // VDIM) * j + lane // VDIM, part, 0.0)
        part = jnp.sum(part, axis=0, keepdims=True)
        for h in range(hubs):
            stage3[h * slot + j : h * slot + j + 1, :] = part
    send3[...] = stage3[...].astype(BF16).reshape(send3.shape)
    each_hub(
        lambda h: launch(
            hub_device(h), send3.at[h], recv3.at[me], link_sem.at[0, 3], link_sem.at[1, 3]
        )
    )
    drain(0, 1, send2)
    drain(0, 2, send2r)

    @pl.when(is_hub)
    def _():
        recv3[me] = send3[my_hub]
        drain(1, 4, wocol.at[pl.ds(0, n * cut)])
        drain(1, 5, wocol.at[pl.ds(0, n * (width - cut))])
        drain(1, 3, recv3)
        flat = stage.at[pl.ds(0, n * slot)]
        flat[...] = recv3[...].astype(F32).reshape(flat.shape)
        rows = [flat[pl.ds(j, n, stride=slot), :].astype(BF16) for j in range(tiles)]
        raw = [flat[pl.ds(tiles + j, n, stride=slot), :] for j in range(per_hub)]
        part = dot(jnp.concatenate(rows, axis=1), wocol[...])
        send4[...] = (jnp.concatenate(raw, axis=1) + part).astype(BF16)

        def spread(k, carry):
            j = lax.rem(2 * k, n) + (2 * k) // n
            peer = upper * j + (1 - upper) * (n - 2 - 2 * (j // 2) + lax.rem(j, 2))

            @pl.when(peer != me)
            def _():
                launch(peer, send4, recv4.at[my_hub], link_sem.at[0, 6], hub_sem.at[my_hub])

            return carry

        lax.fori_loop(0, n, spread, 0)
        recv4[my_hub] = send4[...]

    l_gm.wait()
    l_wg.wait()
    l_wu.wait()
    l_wd.wait()
    half = wg.shape[1] // 2
    parts = [slice(0, half), slice(half, 2 * half)]
    gates = [jnp.zeros((n, half), F32) for _ in parts]
    lifts = [jnp.zeros((n, half), F32) for _ in parts]
    power = jnp.zeros((n, LANES), F32)
    for i in range(hubs):
        h = near_first(i)

        @pl.when(me != hub_device(h))
        def _():
            await_bytes(recv4.at[h], hub_sem.at[h])

        part = recv4[h].astype(F32)
        for j in range(per_hub):
            piece = part[:, j * LANES : (j + 1) * LANES]
            power = power + piece * piece
        gains = [
            part[:, j * LANES : (j + 1) * LANES] * g_moe[pl.ds(h * per_hub + j, 1), :]
            for j in range(per_hub)
        ]
        rows = jnp.concatenate(gains, axis=1).astype(BF16)
        for q, at in enumerate(parts):
            gates[q] = gates[q] + dot(rows, wg[columns(h), at])
            lifts[q] = lifts[q] + dot(rows, wu[columns(h), at])
    scale = lax.rsqrt(jnp.sum(power, axis=1, keepdims=True) * (1.0 / tok.shape[1]) + EPS)
    hidden = [
        (jax.nn.silu(gate * scale) * (lift * scale)).astype(BF16)
        for gate, lift in zip(gates, lifts)
    ]
    result = dot(hidden[0], wd[parts[0], :]) + dot(hidden[1], wd[parts[1], :])
    for j in range(tall):
        stage[pl.ds(j, n, stride=tall), :] = result[:, j * LANES : (j + 1) * LANES]
    send6[...] = stage[pl.ds(0, n * tall), :].astype(BF16).reshape(send6.shape)
    send(7, lambda peer: send6.at[peer], recv6.at[me])
    recv6[me] = send6[me]
    for h in range(hubs):
        part = recv4[h].astype(F32)
        for j in range(per_hub):
            stage[pl.ds(h * per_hub + j, n, stride=tall), :] = part[:, j * LANES : (j + 1) * LANES]
    resid = stage[band(me, tall), :]
    each_hub(lambda h: await_bytes(send3.at[h], link_sem.at[0, 3]))
    for half, size in enumerate((cut, width - cut)):
        each_hub(
            lambda h: await_bytes(wocol.at[pl.ds(0, size)], link_sem.at[0, 4 + half])
        )

    @pl.when(is_hub)
    def _():
        def step(k, carry):
            await_bytes(send4, link_sem.at[0, 6])
            return carry

        lax.fori_loop(1, n, step, 0)

    l_route.wait()
    l_score.wait()
    topk = route.shape[1]
    weight = score[0, 0]
    for k in range(1, topk):
        weight = weight + score[0, k]
    shares = [jnp.full(resid.shape, score[0, k]) / weight for k in range(topk)]
    drain(1, 7, recv6)
    moe_sum = shares[0] * recv6[route[0, 0]].astype(F32)
    for k in range(1, topk):
        moe_sum = moe_sum + shares[k] * recv6[route[0, k]].astype(F32)
    mixed = resid + moe_sum
    for r in range(tall):
        mixed_ref[:, r * LANES : (r + 1) * LANES] = mixed[r : r + 1, :].astype(BF16)
    drain(0, 7, send6)


def finish(mixed, nlat, nrope, mixed_hbm, nlat_hbm, nrope_hbm, sem):
    pairs = [(mixed, mixed_hbm), (nlat, nlat_hbm), (nrope, nrope_hbm)]
    copies = [pltpu.make_async_copy(a, b, sem.at[i]) for i, (a, b) in enumerate(pairs)]
    for copy in copies:
        copy.start()
    for copy in copies:
        copy.wait()


def body(
    tokens, cache_latent, cache_rope, lengths, w_query, w_latent, w_rope, w_absorb, w_value,
    w_output, gain_attn, gain_latent, gain_moe, routes, route_scores, w_gate, w_up, w_down,
):
    n = lax.axis_size("ep")
    d = tokens.shape[1]
    qw, lw = w_query.shape[1], w_latent.shape[1]
    tall, wide = d // LANES, (qw + lw) // LANES
    vmem = pl.BlockSpec(memory_space=pltpu.VMEM)
    hbm = pl.BlockSpec(memory_space=pltpu.HBM)
    lat, gain, moe = (g.reshape(-1, LANES) for g in (gain_latent, gain_attn, gain_moe))

    def like(a):
        return pltpu.VMEM(a.shape[-2:], a.dtype)

    depth = w_query.shape[0]
    turned = depth == LANES
    if turned:
        w_rope = w_rope.T
    hubs = min(n // 4, tall)
    row = lambda count, size: pltpu.VMEM((count, 1, size), F32)
    tile = lambda count, size: pltpu.VMEM((count, size, LANES), BF16)
    outs = (
        jax.ShapeDtypeStruct(tokens.shape, BF16),
        jax.ShapeDtypeStruct((1, lw), BF16),
        jax.ShapeDtypeStruct((1, ROPE), BF16),
    )
    made = pl.pallas_call(
        functools.partial(kernel, n, hubs),
        out_shape=tuple(pltpu.VMEM(o.shape, o.dtype) for o in outs),
        in_specs=[hbm] * 18,
        out_specs=(vmem, vmem, vmem),
        scratch_shapes=[
            like(tokens), like(gain), like(lat), like(moe),
            pltpu.SMEM(lengths.shape, lengths.dtype), pltpu.SMEM(routes.shape, routes.dtype),
            pltpu.SMEM(route_scores.shape, route_scores.dtype),
            like(cache_latent), pltpu.VMEM((LANES, qw), BF16),
            pltpu.VMEM((LANES, lw), BF16), pltpu.VMEM((ROPE, LANES) if turned else (LANES, ROPE), BF16),
            like(w_absorb), like(w_value), like(w_output), like(w_gate), like(w_up), like(w_down),
            pltpu.VMEM((LANES, qw), BF16), pltpu.VMEM((n * w_output.shape[0], d // hubs), BF16),
            pltpu.VMEM((lw + ROPE, cache_latent.shape[1]), BF16), pltpu.VMEM(w_absorb.shape[::-1], BF16),
            pltpu.VMEM((tall, LANES), F32),
            row(tall, LANES), row(n, LANES), pltpu.VMEM((n * max(tall, wide), LANES), F32),
            tile(n, wide), tile(n, wide), pltpu.VMEM((n * EXACT, LANES), F32),
            pltpu.VMEM((n * EXACT, LANES), F32),
            pltpu.VMEM((hubs * 16, LANES), F32), tile(hubs, 16), tile(n, 16),
            pltpu.VMEM((n, d // hubs), BF16), pltpu.VMEM((hubs, n, d // hubs), BF16),
            tile(n, tall), tile(n, tall),
            pltpu.SemaphoreType.DMA((18,)),
            pltpu.SemaphoreType.DMA((2, 8)),
            pltpu.SemaphoreType.DMA((hubs,)),
        ],
        compiler_params=pltpu.CompilerParams(
            collective_id=0, has_side_effects=True, vmem_limit_bytes=56 * 1024 * 1024
        ),
    )(
        tokens, gain, lat, moe, lengths, routes, route_scores, cache_latent, cache_rope, w_query,
        w_latent, w_rope, w_absorb, w_value, w_output, w_gate, w_up, w_down,
    )
    return pl.pallas_call(
        finish,
        out_shape=outs,
        in_specs=[vmem] * 3,
        out_specs=[hbm] * 3,
        scratch_shapes=[pltpu.SemaphoreType.DMA((3,))],
    )(*[pltpu.with_memory_space_constraint(m, pltpu.VMEM) for m in made])


def solution(mesh):
    rows = P(("grp", "ep"), None)
    cube = P(("grp", "ep"), None, None)
    split = P("ep", None)
    placed = (
        rows, cube, cube, P(("grp", "ep")), split, split, split, P(), P(), split, P(), P(), P(),
        rows, rows, P("ep", None, None), P("ep", None, None), P("ep", None, None),
    )
    return jax.shard_map(
        body, mesh=mesh, in_specs=placed, out_specs=(rows, rows, rows), check_vma=False
    )
```

time: 49 us -> 30.3 us (0.62)
  Pallas kernels: 41.5 us -> 28.8 us
  local copies, waits for them, and re-layouts: 5.06 us -> 0 us
  other arithmetic: 0.75 us -> 0 us
    pallas_call x1 -> x2, Pallas kernels: 41.5 us -> 28.8 us  [the longest x1 28.2 us: body(): pl.pallas_call(functools.partial(kernel, n, hubs), out_shape=tuple((pltpu...]
    unnamed x4 -> x0, local copies, waits for them, and re-layouts: 5.06 us -> none
    concatenate x1 -> x0, other arithmetic: 0.65 us -> none  [body(): jnp.concatenate([jnp.concatenate([cosine, cosine], axis=1), jnp.concatena...]
where the time goes in v1:
time: 30.3 us; the launch traced here: 30.1 us
  Pallas kernels  28.8 us (95%)
  between operations  1.29 us (4%)
    pallas_call x1, Pallas kernels, body(): pl.pallas_call(functools.partial(kernel, n, hubs), out_shape=tuple((pltpu...  28.2 us
    pallas_call x1, Pallas kernels, body(): pl.pallas_call(finish, out_shape=outs, in_specs=[vmem] * 3, out_specs=[hb...  0.63 us

profile of v1, /device:TPU:0, one launch (start us, length us, event | category | flops | bytes accessed | tf_op | source)
XLA Modules:
  0.0 30.1 jit_solution(12528666905270519358)
XLA Ops:
  1.3 28.2 %shard_map.193 = (bf16[1,2048]{1,0:T(2,128)(2,1)S(1)}, bf16[1,512]{1,0:T(2,128)(2,1)S(1)}, bf16[1,32]{1,0:T(2,128)(2,1)S(1)}) custom-call(bf16[1,2048]{1,0:T(2,128)(2,1)} %tok_hbm.1, f32[16,128]{1,0:T(8,128)} %bitcast.4, f32[4,128]{1,0:T(4,128)} %bitcast.7, f32[16,128]{1,0:T(8,128)} %bitcast.5, s32[1]{0:T(128)S(6)} %copy.21.len_hbm, s32[1,2]{1,0:T(1,128)} %route_hbm.1, ...), custom_call_target="tpu_custom_call" | custom-call | tf_op jit(solution)/shard_map/pallas_call | solution.py:491
  29.5 0.6 %shard_map.194 = (bf16[1,2048]{1,0:T(2,128)(2,1)}, bf16[1,512]{1,0:T(2,128)(2,1)}, bf16[1,32]{1,0:T(2,128)(2,1)}) custom-call(bf16[1,2048]{1,0:T(2,128)(2,1)S(1)} %get-tuple-element.6.mixed, bf16[1,512]{1,0:T(2,128)(2,1)S(1)} %get-tuple-element.7.nlat, bf16[1,32]{1,0:T(2,128)(2,1)S(1)} %get-tuple-element.8.nrope), custom_call_target="tpu_custom_call" | custom-call | tf_op jit(solution)/shard_map/pallas_call | solution.py:523
